TPU v7x, 1024 devices: a 2x16x16 block of a 4x16x16 slice. The times are simulated.
1024 devices in a mesh: grp: 2 (over x), sp: 16 (over z), tp: 32 (over y, core).
Axes of the slice: x: 2, y: 16, z: 16, core: 2. Of those that a mesh axis runs over, the one named last changes fastest.
The devices are a block of a 4x16x16 slice.
Arguments:
- grid_tokens: bfloat16 [256, 512, 1024], P(('grp', 'sp'), 'tp'), parts along dimension 0, may hold values from -6 to 6
- norm_gain: float32 [2, 1024], replicated, may hold values from 0.1 to 1.9
- w_query: bfloat16 [2, 1024, 512], replicated, may hold values from -0.84375 to 0.84375
- w_key: bfloat16 [2, 1024, 512], replicated, may hold values from -1.1390625 to 1.1390625
- w_value: bfloat16 [2, 1024, 512], replicated, may hold values from -0.1875 to 0.1875
- offset_bias: float32 [2, 4, 15, 31], replicated, may hold values from -5 to 5
- w_out: bfloat16 [2, 512, 1024], replicated, may hold values from -1 to 1
Outputs:
- grid_out: bfloat16 [256, 512, 1024], P(('grp', 'sp'), 'tp'), parts along dimension 0
There are 2 independent parts, one for each index of `grp`. A program takes and returns all parts, laid end to end along the dimension named above; an argument that names none is the same for every part. Nothing has to cross between parts.
All inputs are finite; a program needn't handle non-finite values.
Results may differ from a plain program's by a relative error of at most 0.014.
Values may be sent and summed in bfloat16 or wider, within the bound.
No kernel may reach another device: no remote copies, remote signals or barrier semaphores. Data moves between devices by JAX's collectives and lax.ppermute only.
A program may use at most 64 MiB of HBM per device.

v0:
```python
import functools
import math

import jax
import jax.numpy as jnp
from jax import lax
from jax.experimental import pallas as pl
from jax.experimental.pallas import tpu as pltpu
from jax.sharding import PartitionSpec as P

HEAD_DIM = 128
WIN_ROWS = 8
WIN_COLS = 16
LAYERS = 2
HALF_ROWS = WIN_ROWS // 2
HALF_COLS = WIN_COLS // 2

NORM_EPSILON = 1e-06
LOG2E = math.log2(math.e)
MASKED = -1e30

BLOCK_ROWS = 8
BLOCK_COLS = 16
SLAB_ROWS = BLOCK_ROWS + WIN_ROWS
SLAB_COLS = BLOCK_COLS + WIN_COLS
QUERIES = BLOCK_ROWS * BLOCK_COLS
SLAB = SLAB_ROWS * SLAB_COLS
LANES = 128
GROUP = LANES // SLAB_COLS
SPAN = SLAB_ROWS - GROUP + BLOCK_ROWS
BLOCKS = 5

TILES = 3
SLOTS = 3
CHUNK = 32

ORDER = ((0, -1), (-1, 0), (-1, -1), (-1, 1), (1, -1), (1, 0), (1, 1), (0, 1))

VMEM = pl.BlockSpec(memory_space=pltpu.VMEM)
HBM = pl.BlockSpec(memory_space=pltpu.HBM)


def bias_kernel(grid_rows, grid_cols, tile_rows, tile_cols, table, out_ref, lines, shifted):
    layers, offsets, heads = table.shape[:3]
    first_row = lax.axis_index("sp") * tile_rows
    first_col = lax.axis_index("tp") * tile_cols

    blank = jnp.zeros((heads, LANES - table.shape[3]), jnp.float32)
    for layer in range(layers):
        rows = [
            jnp.concatenate((table[layer, o] * LOG2E, blank), axis=1) for o in range(offsets)
        ]
        turned = [[pltpu.roll(row, g * SLAB_COLS, 1) if g else row for row in rows] for g in range(GROUP)]
        for u in range(SPAN):
            line = jnp.zeros((heads, LANES), jnp.float32)
            for g in range(GROUP):
                if 0 <= u + g - HALF_ROWS < offsets:
                    line = line + turned[g][u + g - HALF_ROWS]
            lines[layer, u] = line
        for head in range(heads):
            for u in range(SPAN):
                shifted[layer, head, u] = pltpu.roll(
                    jnp.broadcast_to(lines[layer, u, head : head + 1], (BLOCK_COLS, LANES)),
                    LANES - (HALF_COLS - 1),
                    1,
                    stride=1,
                    stride_axis=0,
                )

    lane = lax.broadcasted_iota(jnp.int32, (BLOCK_COLS, LANES), 1)
    column = lax.broadcasted_iota(jnp.int32, (BLOCK_COLS, LANES), 0)
    key_col = lane % SLAB_COLS
    key_row = lane // SLAB_COLS

    def block(index, _):
        last = index // (BLOCKS - 1)
        row_block, col_block = (index // 2) % 2, index % 2
        row0 = first_row + (1 - last) * (row_block * BLOCK_ROWS - HALF_ROWS)
        col0 = first_col + (1 - last) * (col_block * BLOCK_COLS - HALF_COLS)
        col_start = jnp.clip(col0 + column - HALF_COLS, 0, grid_cols - WIN_COLS)
        behind = col0 - HALF_COLS + key_col - col_start
        col_inside = (behind >= 0) & (behind < WIN_COLS)
        for i in range(BLOCK_ROWS):
            row_start = jnp.clip(row0 + i - HALF_ROWS, 0, grid_rows - WIN_ROWS)
            for j in range(SLAB_ROWS // GROUP):
                below = key_row + (row0 - HALF_ROWS + j * GROUP - row_start)
                inside = col_inside & (below >= 0) & (below < WIN_ROWS)
                for head in range(heads):
                    out_ref[
                        index,
                        head,
                        i * BLOCK_COLS : (i + 1) * BLOCK_COLS,
                        j * LANES : (j + 1) * LANES,
                    ] = jnp.where(
                        inside, shifted[last, head, GROUP * j - i + BLOCK_ROWS - 1], MASKED
                    )
        return 0

    lax.fori_loop(0, BLOCKS, block, 0)


def normed_rows(values, gain):
    factor = lax.rsqrt(jnp.mean(values * values, axis=-1, keepdims=True) + NORM_EPSILON)
    return values * factor * gain


def project(cells, weight):
    rows, cols, width = cells.shape
    out = jnp.dot(
        cells.reshape(rows * cols, width), weight, preferred_element_type=jnp.float32
    )
    return out.astype(jnp.bfloat16).reshape(rows, cols, weight.shape[1])


def layers_kernel(*refs):
    tiles, refs = refs[: TILES * TILES], refs[TILES * TILES :]
    gain, query_source, w_key, w_value, out_source, bias, out_ref = refs[:7]
    normed, normed_q, keys, values, queries, mixture, branch, center, scores, weights = refs[7:17]
    w_query, w_out, arrivals = refs[17:]
    loads = [
        pltpu.make_async_copy(query_source, w_query, arrivals.at[0]),
        pltpu.make_async_copy(out_source, w_out, arrivals.at[1]),
    ]
    for load in loads:
        load.start()
    f32, bf16 = jnp.float32, jnp.bfloat16
    heads = w_query.shape[2] // HEAD_DIM
    rows, cols = normed.shape[:2]
    region_rows, region_cols = mixture.shape[:2]
    slots = scores.shape[0]

    def put_values(where, out):
        for head in range(heads):
            values[(*where, pl.ds(2 * head * HEAD_DIM, HEAD_DIM))] = out[
                :, :, head * HEAD_DIM : (head + 1) * HEAD_DIM
            ]

    def attend(units):
        def products(step):
            _, head, tile, slab = units[step]
            lanes = pl.ds(head * HEAD_DIM, HEAD_DIM)
            scores[step % slots] = lax.dot_general(
                queries[(*tile, lanes)].reshape(QUERIES, HEAD_DIM),
                keys[(*slab, lanes)].reshape(SLAB, HEAD_DIM),
                (((1,), (1,)), ((), ())),
                preferred_element_type=f32,
            )

        def softmax(step):
            block, head, _, _ = units[step]
            for first in range(0, QUERIES, CHUNK):
                part = pl.ds(first, CHUNK)
                shifted = scores[step % slots, part] * (LOG2E / HEAD_DIM**0.5)
                shifted = shifted + bias[block, head, part]
                top = jnp.max(shifted, axis=1, keepdims=True)
                weights[step % slots, part] = jnp.exp2(shifted - top).astype(bf16)

        def mix(step):
            _, head, tile, slab = units[step]
            both = jnp.dot(
                weights[step % slots],
                values[(*slab, pl.ds(2 * head * HEAD_DIM, 2 * HEAD_DIM))].reshape(
                    SLAB, 2 * HEAD_DIM
                ),
                preferred_element_type=f32,
            )
            out = (both[:, :HEAD_DIM] / both[:, HEAD_DIM:]).astype(bf16)
            mixture[(*tile, pl.ds(head * HEAD_DIM, HEAD_DIM))] = out.reshape(
                BLOCK_ROWS, BLOCK_COLS, HEAD_DIM
            )

        for step in range(len(units) + 2):
            if step < len(units):
                products(step)
            if 0 <= step - 1 < len(units):
                softmax(step - 1)
            if 0 <= step - 2:
                mix(step - 2)

    def part_of(r, c):
        return tiles[r // BLOCK_ROWS * TILES + c][r % BLOCK_ROWS].astype(f32)

    for head in range(heads):
        values[:, :, pl.ds((2 * head + 1) * HEAD_DIM, HEAD_DIM)] = jnp.ones(
            (rows, cols, HEAD_DIM), bf16
        )
    for r in range(rows):
        parts = [normed_rows(part_of(r, c), gain[0:1]) for c in range(TILES)]
        for index, part in enumerate(parts):
            normed[r, index * BLOCK_COLS : (index + 1) * BLOCK_COLS] = part.astype(bf16)
        if 0 <= r - HALF_ROWS < region_rows:
            for index in range(2):
                both = (parts[index][HALF_COLS:], parts[index + 1][:HALF_COLS])
                normed_q[r - HALF_ROWS, index * BLOCK_COLS : (index + 1) * BLOCK_COLS] = (
                    jnp.concatenate(both, axis=0).astype(bf16)
                )
        if r % BLOCK_ROWS == BLOCK_ROWS - 1:
            band = pl.ds(r + 1 - BLOCK_ROWS, BLOCK_ROWS)
            keys[band] = project(normed[band], w_key[0])
            put_values((band, slice(None)), project(normed[band], w_value[0]))
    for load in loads:
        load.wait()
    queries[...] = project(normed_q[...], w_query[0])

    units = []
    for index in range(BLOCKS - 1):
        row, col = index // 2 * BLOCK_ROWS, index % 2 * BLOCK_COLS
        tile = (pl.ds(row, BLOCK_ROWS), pl.ds(col, BLOCK_COLS))
        slab = (pl.ds(row, SLAB_ROWS), pl.ds(col, SLAB_COLS))
        units += [(index, head, tile, slab) for head in range(heads)]
    attend(units)
    branch[...] = jnp.dot(
        mixture[...].reshape(region_rows * region_cols, heads * HEAD_DIM),
        w_out[0],
        preferred_element_type=f32,
    ).reshape(branch.shape)

    own = pl.ds(HALF_ROWS, BLOCK_ROWS)
    inner = slice(HALF_COLS, HALF_COLS + BLOCK_COLS)
    for r in range(region_rows):
        before, here, after = (part_of(r + HALF_ROWS, c) for c in range(TILES))
        tokens = jnp.concatenate((before[HALF_COLS:], here, after[:HALF_COLS]), axis=0)
        stream = (tokens + branch[r]).astype(bf16).astype(f32)
        part = normed_rows(stream, gain[1:2])
        normed[r, :region_cols] = part.astype(bf16)
        if 0 <= r - HALF_ROWS < BLOCK_ROWS:
            normed_q[r - HALF_ROWS, :BLOCK_COLS] = part[inner].astype(bf16)
            center[r - HALF_ROWS] = stream[inner]
    region = (pl.ds(0, region_rows), pl.ds(0, region_cols))
    tile = (pl.ds(0, BLOCK_ROWS), pl.ds(0, BLOCK_COLS))
    keys[region] = project(normed[region], w_key[1])
    put_values(region, project(normed[region], w_value[1]))
    queries[tile] = project(normed_q[tile], w_query[1])
    attend([(BLOCKS - 1, head, tile, region) for head in range(heads)])
    last = jnp.dot(
        mixture[tile].reshape(QUERIES, heads * HEAD_DIM), w_out[1], preferred_element_type=f32
    )
    out_ref[...] = (center[...] + last.reshape(out_ref.shape)).astype(out_ref.dtype)


def from_offset(cells, row, col):
    rows, cols = lax.axis_size("sp"), lax.axis_size("tp")
    pairs = [
        ((r + row) * cols + c + col, r * cols + c)
        for r in range(rows)
        for c in range(cols)
        if 0 <= r + row < rows and 0 <= c + col < cols
    ]
    return lax.ppermute(cells, ("sp", "tp"), pairs)


def on_device(grid_tokens, norm_gain, w_query, w_key, w_value, offset_bias, w_out):
    tile_rows, tile_cols, width = grid_tokens.shape
    grid_rows = tile_rows * lax.axis_size("sp")
    grid_cols = tile_cols * lax.axis_size("tp")
    heads = offset_bias.shape[1]
    inner = heads * HEAD_DIM
    bf16, f32 = jnp.bfloat16, jnp.float32

    bias = pl.pallas_call(
        functools.partial(bias_kernel, grid_rows, grid_cols, tile_rows, tile_cols),
        out_shape=jax.ShapeDtypeStruct((BLOCKS, heads, QUERIES, SLAB), f32),
        in_specs=[VMEM],
        out_specs=VMEM,
        scratch_shapes=[
            pltpu.VMEM((LAYERS, SPAN, heads, LANES), f32),
            pltpu.VMEM((LAYERS, heads, SPAN, BLOCK_COLS, LANES), f32),
        ],
        compiler_params=pltpu.CompilerParams(vmem_limit_bytes=8 * 2**20),
        cost_estimate=pl.CostEstimate(flops=4 * 10**6, bytes_accessed=32 * 2**20, transcendentals=0),
        name="bias",
    )(jnp.transpose(offset_bias, (0, 2, 1, 3)))

    arrived = {(0, 0): grid_tokens}
    for offset in ORDER:
        arrived[offset] = from_offset(grid_tokens, *offset)
    tiles = [arrived[(row, col)] for row in (-1, 0, 1) for col in (-1, 0, 1)]

    rows, cols = TILES * tile_rows, TILES * tile_cols
    region_rows, region_cols = 2 * tile_rows, 2 * tile_cols
    return pl.pallas_call(
        layers_kernel,
        out_shape=jax.ShapeDtypeStruct(grid_tokens.shape, grid_tokens.dtype),
        in_specs=[VMEM] * (len(tiles) + 1) + [HBM, VMEM, VMEM, HBM, VMEM],
        out_specs=VMEM,
        scratch_shapes=[
            pltpu.VMEM((rows, cols, width), bf16),
            pltpu.VMEM((region_rows, region_cols, width), bf16),
            pltpu.VMEM((rows, cols, inner), bf16),
            pltpu.VMEM((rows, cols, 2 * inner), bf16),
            pltpu.VMEM((region_rows, region_cols, inner), bf16),
            pltpu.VMEM((region_rows, region_cols, inner), bf16),
            pltpu.VMEM((region_rows, region_cols, width), f32),
            pltpu.VMEM((tile_rows, tile_cols, width), f32),
            pltpu.VMEM((SLOTS, QUERIES, SLAB), f32),
            pltpu.VMEM((SLOTS, QUERIES, SLAB), bf16),
            pltpu.VMEM(w_query.shape, bf16),
            pltpu.VMEM(w_out.shape, bf16),
            pltpu.SemaphoreType.DMA((2,)),
        ],
        compiler_params=pltpu.CompilerParams(vmem_limit_bytes=24 * 2**20),
        cost_estimate=pl.CostEstimate(
            flops=6 * 10**9, bytes_accessed=16 * 2**20, transcendentals=10**6
        ),
        name="layers",
    )(
        *tiles,
        norm_gain,
        pltpu.with_memory_space_constraint(w_query, pltpu.HBM),
        w_key,
        w_value,
        pltpu.with_memory_space_constraint(w_out, pltpu.HBM),
        bias,
    )


def solution(mesh):
    return jax.shard_map(
        on_device,
        mesh=mesh,
        in_specs=(P(("grp", "sp"), "tp", None), P(), P(), P(), P(), P(), P()),
        out_specs=P(("grp", "sp"), "tp", None),
        check_vma=False,
    )
```

profile of v0, /device:TPU:5, one launch (start us, length us, event | category | flops | bytes accessed | tf_op | source)
XLA Modules:
  0.0 117.1 jit_solution(9869440259631730925)
XLA Ops:
  0.0 1.3 %collective-permute-start.6 = (bf16[8,16,1024]{2,1,0:T(8,128)(2,1)}, bf16[8,16,1024]{2,1,0:T(8,128)(2,1)S(1)}, u32[]{:S(2)}, u32[]{:S(2)}) collective-permute-start(bf16[8,16,1024]{2,1,0:T(8,128)(2,1)} %refs_4_.1), channel_id=1, source_target_pairs={{32,0},{33,1},{34,2},{35,3},{36,4},{37,5},{38,6},{39,7},{40,8},{41... | collective-permute-start | bytes 786440 | tf_op jit(solution)/shard_map/ppermute | solution.py:249
  1.3 1.3 %collective-permute-start.5 = (bf16[8,16,1024]{2,1,0:T(8,128)(2,1)}, bf16[8,16,1024]{2,1,0:T(8,128)(2,1)S(1)}, u32[]{:S(2)}, u32[]{:S(2)}) collective-permute-start(bf16[8,16,1024]{2,1,0:T(8,128)(2,1)} %refs_4_.1), channel_id=1, source_target_pairs={{32,1},{33,2},{34,3},{35,4},{36,5},{37,6},{38,7},{39,8},{40,9},{41... | collective-permute-start | bytes 786440 | tf_op jit(solution)/shard_map/ppermute | solution.py:249
  2.6 84.8 %collective-permute-start.4 = (bf16[8,16,1024]{2,1,0:T(8,128)(2,1)}, bf16[8,16,1024]{2,1,0:T(8,128)(2,1)S(1)}, u32[]{:S(2)}, u32[]{:S(2)}) collective-permute-start(bf16[8,16,1024]{2,1,0:T(8,128)(2,1)} %refs_4_.1), channel_id=1, source_target_pairs={{1,0},{2,1},{3,2},{4,3},{5,4},{6,5},{7,6},{8,7},{9,8},{10,9},{11,1... | collective-permute-start | bytes 786440 | tf_op jit(solution)/shard_map/ppermute | solution.py:249
  87.4 2.0 %collective-permute-start.3 = (bf16[8,16,1024]{2,1,0:T(8,128)(2,1)}, bf16[8,16,1024]{2,1,0:T(8,128)(2,1)S(1)}, u32[]{:S(2)}, u32[]{:S(2)}) collective-permute-start(bf16[8,16,1024]{2,1,0:T(8,128)(2,1)} %refs_4_.1), channel_id=1, source_target_pairs={{0,1},{1,2},{2,3},{3,4},{4,5},{5,6},{6,7},{7,8},{8,9},{9,10},{10,1... | collective-permute-start | bytes 786440 | tf_op jit(solution)/shard_map/ppermute | solution.py:249
  89.4 5.4 %collective-permute-start.2 = (bf16[8,16,1024]{2,1,0:T(8,128)(2,1)}, bf16[8,16,1024]{2,1,0:T(8,128)(2,1)S(1)}, u32[]{:S(2)}, u32[]{:S(2)}) collective-permute-start(bf16[8,16,1024]{2,1,0:T(8,128)(2,1)} %refs_4_.1), channel_id=1, source_target_pairs={{1,32},{2,33},{3,34},{4,35},{5,36},{6,37},{7,38},{8,39},{9,40},{10... | collective-permute-start | bytes 786440 | tf_op jit(solution)/shard_map/ppermute | solution.py:249
  94.7 0.0 collective-permute-done.6.refs_7_
  94.7 1.6 %collective-permute-start.1 = (bf16[8,16,1024]{2,1,0:T(8,128)(2,1)}, bf16[8,16,1024]{2,1,0:T(8,128)(2,1)S(1)}, u32[]{:S(2)}, u32[]{:S(2)}) collective-permute-start(bf16[8,16,1024]{2,1,0:T(8,128)(2,1)} %refs_4_.1), channel_id=1, source_target_pairs={{0,32},{1,33},{2,34},{3,35},{4,36},{5,37},{6,38},{7,39},{8,40},{9,... | collective-permute-start | bytes 786440 | tf_op jit(solution)/shard_map/ppermute | solution.py:249
  96.3 0.0 collective-permute-done.5.refs_6_
  96.3 1.3 %collective-permute-start = (bf16[8,16,1024]{2,1,0:T(8,128)(2,1)}, bf16[8,16,1024]{2,1,0:T(8,128)(2,1)S(1)}, u32[]{:S(2)}, u32[]{:S(2)}) collective-permute-start(bf16[8,16,1024]{2,1,0:T(8,128)(2,1)} %refs_4_.1), channel_id=1, source_target_pairs={{0,33},{1,34},{2,35},{3,36},{4,37},{5,38},{6,39},{7,40},{8,41},{9,... | collective-permute-start | bytes 786440 | tf_op jit(solution)/shard_map/ppermute | solution.py:249
  97.6 0.0 collective-permute-done.4.refs_5_
  97.7 1.3 %collective-permute-start.7 = (bf16[8,16,1024]{2,1,0:T(8,128)(2,1)}, bf16[8,16,1024]{2,1,0:T(8,128)(2,1)S(1)}, u32[]{:S(2)}, u32[]{:S(2)}) collective-permute-start(bf16[8,16,1024]{2,1,0:T(8,128)(2,1)} %refs_4_.1), channel_id=1, source_target_pairs={{33,0},{34,1},{35,2},{36,3},{37,4},{38,5},{39,6},{40,7},{41,8},{42... | collective-permute-start | bytes 786440 | tf_op jit(solution)/shard_map/ppermute | solution.py:249
  99.0 0.0 copy-start
  99.0 0.8 copy-done
  99.8 0.0 copy-start.1
  99.8 0.0 copy-start.2
  99.8 0.0 copy-start.3
  99.8 0.0 copy-start.4
  99.8 1.2 %bias.1.refs_14_ = f32[5,4,128,512]{3,2,1,0:T(8,128)S(1)} custom-call(f32[2,15,4,31]{3,2,1,0:T(4,128)S(1)} %bitcast.1), custom_call_target="tpu_custom_call" | custom-call | flops 4000000 | bytes 33554432 | tf_op jit(solution)/shard_map/bias/pallas_call | solution.py:260
  101.1 0.0 collective-permute-done.3.refs_3_
  101.1 1.7 %collective-permute-done.2.refs_2_ = bf16[8,16,1024]{2,1,0:T(8,128)(2,1)S(1)} collective-permute-done((bf16[8,16,1024]{2,1,0:T(8,128)(2,1)}, bf16[8,16,1024]{2,1,0:T(8,128)(2,1)S(1)}, u32[]{:S(2)}, u32[]{:S(2)}) %collective-permute-start.2) | collective-permute-done | bytes 262176 | tf_op jit(solution)/shard_map/ppermute | solution.py:249
  102.8 5.6 %collective-permute-done.1.refs_1_ = bf16[8,16,1024]{2,1,0:T(8,128)(2,1)S(1)} collective-permute-done((bf16[8,16,1024]{2,1,0:T(8,128)(2,1)}, bf16[8,16,1024]{2,1,0:T(8,128)(2,1)S(1)}, u32[]{:S(2)}, u32[]{:S(2)}) %collective-permute-start.1) | collective-permute-done | bytes 262176 | tf_op jit(solution)/shard_map/ppermute | solution.py:249
  108.4 0.0 collective-permute-done.refs_0_
  108.4 0.0 collective-permute-done.7.refs_8_
  108.4 0.0 copy-done.1
  108.4 0.0 copy-done.2
  108.4 0.0 copy-done.3
  108.4 0.0 copy-done.4
  108.4 8.7 %layers.1 = bf16[8,16,1024]{2,1,0:T(8,128)(2,1)} custom-call(bf16[8,16,1024]{2,1,0:T(8,128)(2,1)S(1)} %collective-permute-done.refs_0_, bf16[8,16,1024]{2,1,0:T(8,128)(2,1)S(1)} %collective-permute-done.1.refs_1_, bf16[8,16,1024]{2,1,0:T(8,128)(2,1)S(1)} %collective-permute-done.2.refs_2_, bf16[8,16,1024]{2,1,0:T(8,128)(2,1)S(1)} %collective-permute-done.3.refs_3_, ...), custom_call_target="tpu_custom_call" | custom-call | flops 6000000000 | bytes 16777216 | tf_op jit(solution)/shard_map/layers/pallas_call | solution.py:281
Async XLA Ops:
  0.0 94.7 %collective-permute-start.6 = (bf16[8,16,1024]{2,1,0:T(8,128)(2,1)}, bf16[8,16,1024]{2,1,0:T(8,128)(2,1)S(1)}, u32[]{:S(2)}, u32[]{:S(2)}) collective-permute-start(bf16[8,16,1024]{2,1,0:T(8,128)(2,1)} %refs_4_.1), channel_id=1, source_target_pairs={{32,0},{33,1},{34,2},{35,3},{36,4},{37,5},{38,6},{39,7},{40,8},{41... | collective-permute-start | bytes 786440 | tf_op jit(solution)/shard_map/ppermute | solution.py:249
  1.3 95.0 %collective-permute-start.5 = (bf16[8,16,1024]{2,1,0:T(8,128)(2,1)}, bf16[8,16,1024]{2,1,0:T(8,128)(2,1)S(1)}, u32[]{:S(2)}, u32[]{:S(2)}) collective-permute-start(bf16[8,16,1024]{2,1,0:T(8,128)(2,1)} %refs_4_.1), channel_id=1, source_target_pairs={{32,1},{33,2},{34,3},{35,4},{36,5},{37,6},{38,7},{39,8},{40,9},{41... | collective-permute-start | bytes 786440 | tf_op jit(solution)/shard_map/ppermute | solution.py:249
  2.6 95.0 %collective-permute-start.4 = (bf16[8,16,1024]{2,1,0:T(8,128)(2,1)}, bf16[8,16,1024]{2,1,0:T(8,128)(2,1)S(1)}, u32[]{:S(2)}, u32[]{:S(2)}) collective-permute-start(bf16[8,16,1024]{2,1,0:T(8,128)(2,1)} %refs_4_.1), channel_id=1, source_target_pairs={{1,0},{2,1},{3,2},{4,3},{5,4},{6,5},{7,6},{8,7},{9,8},{10,9},{11,1... | collective-permute-start | bytes 786440 | tf_op jit(solution)/shard_map/ppermute | solution.py:249
  87.4 13.7 %collective-permute-start.3 = (bf16[8,16,1024]{2,1,0:T(8,128)(2,1)}, bf16[8,16,1024]{2,1,0:T(8,128)(2,1)S(1)}, u32[]{:S(2)}, u32[]{:S(2)}) collective-permute-start(bf16[8,16,1024]{2,1,0:T(8,128)(2,1)} %refs_4_.1), channel_id=1, source_target_pairs={{0,1},{1,2},{2,3},{3,4},{4,5},{5,6},{6,7},{7,8},{8,9},{9,10},{10,1... | collective-permute-start | bytes 786440 | tf_op jit(solution)/shard_map/ppermute | solution.py:249
  89.4 13.4 %collective-permute-start.2 = (bf16[8,16,1024]{2,1,0:T(8,128)(2,1)}, bf16[8,16,1024]{2,1,0:T(8,128)(2,1)S(1)}, u32[]{:S(2)}, u32[]{:S(2)}) collective-permute-start(bf16[8,16,1024]{2,1,0:T(8,128)(2,1)} %refs_4_.1), channel_id=1, source_target_pairs={{1,32},{2,33},{3,34},{4,35},{5,36},{6,37},{7,38},{8,39},{9,40},{10... | collective-permute-start | bytes 786440 | tf_op jit(solution)/shard_map/ppermute | solution.py:249
  94.7 13.6 %collective-permute-start.1 = (bf16[8,16,1024]{2,1,0:T(8,128)(2,1)}, bf16[8,16,1024]{2,1,0:T(8,128)(2,1)S(1)}, u32[]{:S(2)}, u32[]{:S(2)}) collective-permute-start(bf16[8,16,1024]{2,1,0:T(8,128)(2,1)} %refs_4_.1), channel_id=1, source_target_pairs={{0,32},{1,33},{2,34},{3,35},{4,36},{5,37},{6,38},{7,39},{8,40},{9,... | collective-permute-start | bytes 786440 | tf_op jit(solution)/shard_map/ppermute | solution.py:249
  96.3 12.1 %collective-permute-start = (bf16[8,16,1024]{2,1,0:T(8,128)(2,1)}, bf16[8,16,1024]{2,1,0:T(8,128)(2,1)S(1)}, u32[]{:S(2)}, u32[]{:S(2)}) collective-permute-start(bf16[8,16,1024]{2,1,0:T(8,128)(2,1)} %refs_4_.1), channel_id=1, source_target_pairs={{0,33},{1,34},{2,35},{3,36},{4,37},{5,38},{6,39},{7,40},{8,41},{9,... | collective-permute-start | bytes 786440 | tf_op jit(solution)/shard_map/ppermute | solution.py:249
  97.7 10.7 %collective-permute-start.7 = (bf16[8,16,1024]{2,1,0:T(8,128)(2,1)}, bf16[8,16,1024]{2,1,0:T(8,128)(2,1)S(1)}, u32[]{:S(2)}, u32[]{:S(2)}) collective-permute-start(bf16[8,16,1024]{2,1,0:T(8,128)(2,1)} %refs_4_.1), channel_id=1, source_target_pairs={{33,0},{34,1},{35,2},{36,3},{37,4},{38,5},{39,6},{40,7},{41,8},{42... | collective-permute-start | bytes 786440 | tf_op jit(solution)/shard_map/ppermute | solution.py:249
  99.0 0.8 copy-start
  99.8 8.6 %copy-start.1 = (bf16[2,1024,512]{2,1,0:T(8,128)(2,1)S(1)}, bf16[2,1024,512]{2,1,0:T(8,128)(2,1)}, u32[]{:S(2)}) copy-start(bf16[2,1024,512]{2,1,0:T(8,128)(2,1)} %refs_11_.1) | copy-start | bytes 6291460
  99.8 8.6 %copy-start.2 = (bf16[2,1024,512]{2,1,0:T(8,128)(2,1)S(1)}, bf16[2,1024,512]{2,1,0:T(8,128)(2,1)}, u32[]{:S(2)}) copy-start(bf16[2,1024,512]{2,1,0:T(8,128)(2,1)} %refs_12_.1) | copy-start | bytes 6291460
  99.8 8.6 %copy-start.3 = (bf16[8,16,1024]{2,1,0:T(8,128)(2,1)S(1)}, bf16[8,16,1024]{2,1,0:T(8,128)(2,1)}, u32[]{:S(2)}) copy-start(bf16[8,16,1024]{2,1,0:T(8,128)(2,1)} %refs_4_.1) | copy-start | bytes 786436
  99.8 8.6 %copy-start.4 = (f32[2,1024]{1,0:T(2,128)S(1)}, f32[2,1024]{1,0:T(2,128)}, u32[]{:S(2)}) copy-start(f32[2,1024]{1,0:T(2,128)} %refs_9_.1) | copy-start | bytes 24580
where the time goes:
time: 117 us
  starting transfers between devices  98.9 us (85%)
  Pallas kernels  9.9 us (8%)
  waiting for transfers between devices  7.34 us (6%)
    ppermute x8, starting transfers between devices, from_offset(): return lax.ppermute(cells, ('sp', 'tp'), pairs)  98.9 us
    pallas_call x1, Pallas kernels, on_device(): pl.pallas_call(layers_kernel, out_shape=jax.ShapeDtypeStruct(grid_tokens....  8.66 us
    ppermute x8, waiting for transfers between devices, from_offset(): return lax.ppermute(cells, ('sp', 'tp'), pairs)  7.34 us
  transfers between devices with their start and end apart: 8, of which 2 were waited for; matrix products, arithmetic and copies ran while one was open for 0% of the time, Pallas kernels for 1%

commit v1 on v0

--- a/solution.py
+++ b/solution.py
@@ -40,10 +40,14 @@
 HBM = pl.BlockSpec(memory_space=pltpu.HBM)
 
 
-def bias_kernel(grid_rows, grid_cols, tile_rows, tile_cols, table, out_ref, lines, shifted):
+def fill_bias(grid, table_source, table, lines, shifted, out_ref, arrival):
+    grid_rows, grid_cols, tile_rows, tile_cols = grid
     layers, offsets, heads = table.shape[:3]
     first_row = lax.axis_index("sp") * tile_rows
     first_col = lax.axis_index("tp") * tile_cols
+    load = pltpu.make_async_copy(table_source, table, arrival)
+    load.start()
+    load.wait()
 
     blank = jnp.zeros((heads, LANES - table.shape[3]), jnp.float32)
     for layer in range(layers):
@@ -99,6 +103,19 @@
     lax.fori_loop(0, BLOCKS, block, 0)
 
 
+def at_corner():
+    return (lax.axis_index("sp") == 0) & (lax.axis_index("tp") == 0)
+
+
+def bias_kernel(grid, table_source, out_ref, filled, table, lines, shifted, arrival):
+    @pl.when(jnp.logical_not(at_corner()))
+    def _():
+        fill_bias(grid, table_source, table, lines, shifted, filled, arrival.at[0])
+        store = pltpu.make_async_copy(filled, out_ref, arrival.at[0])
+        store.start()
+        store.wait()
+
+
 def normed_rows(values, gain):
     factor = lax.rsqrt(jnp.mean(values * values, axis=-1, keepdims=True) + NORM_EPSILON)
     return values * factor * gain
@@ -112,12 +129,13 @@
     return out.astype(jnp.bfloat16).reshape(rows, cols, weight.shape[1])
 
 
-def layers_kernel(*refs):
+def layers_kernel(grid, *refs):
     tiles, refs = refs[: TILES * TILES], refs[TILES * TILES :]
-    gain, query_source, w_key, w_value, out_source, bias, out_ref = refs[:7]
-    normed, normed_q, keys, values, queries, mixture, branch, center, scores, weights = refs[7:17]
-    w_query, w_out, arrivals = refs[17:]
+    gain, query_source, w_key, w_value, out_source, table_source, bias_source, out_ref = refs[:8]
+    normed, normed_q, keys, values, queries, mixture, branch, center, scores, weights = refs[8:18]
+    w_query, w_out, bias, table, lines, shifted, arrivals = refs[18:]
     loads = [
+        pltpu.make_async_copy(bias_source, bias, arrivals.at[2]),
         pltpu.make_async_copy(query_source, w_query, arrivals.at[0]),
         pltpu.make_async_copy(out_source, w_out, arrivals.at[1]),
     ]
@@ -200,6 +218,11 @@
             put_values((band, slice(None)), project(normed[band], w_value[0]))
     for load in loads:
         load.wait()
+
+    @pl.when(at_corner())
+    def _():
+        fill_bias(grid, table_source, table, lines, shifted, bias, arrivals.at[0])
+
     queries[...] = project(normed_q[...], w_query[0])
 
     units = []
@@ -257,19 +280,29 @@
     inner = heads * HEAD_DIM
     bf16, f32 = jnp.bfloat16, jnp.float32
 
+    grid = (grid_rows, grid_cols, tile_rows, tile_cols)
+    table = pltpu.with_memory_space_constraint(
+        jnp.transpose(offset_bias, (0, 2, 1, 3)), pltpu.HBM
+    )
+    bias_shape = (BLOCKS, heads, QUERIES, SLAB)
+    bias_scratch = [
+        pltpu.VMEM(bias_shape, f32),
+        pltpu.VMEM(table.shape, f32),
+        pltpu.VMEM((LAYERS, SPAN, heads, LANES), f32),
+        pltpu.VMEM((LAYERS, heads, SPAN, BLOCK_COLS, LANES), f32),
+    ]
     bias = pl.pallas_call(
-        functools.partial(bias_kernel, grid_rows, grid_cols, tile_rows, tile_cols),
-        out_shape=jax.ShapeDtypeStruct((BLOCKS, heads, QUERIES, SLAB), f32),
-        in_specs=[VMEM],
-        out_specs=VMEM,
-        scratch_shapes=[
-            pltpu.VMEM((LAYERS, SPAN, heads, LANES), f32),
-            pltpu.VMEM((LAYERS, heads, SPAN, BLOCK_COLS, LANES), f32),
-        ],
-        compiler_params=pltpu.CompilerParams(vmem_limit_bytes=8 * 2**20),
-        cost_estimate=pl.CostEstimate(flops=4 * 10**6, bytes_accessed=32 * 2**20, transcendentals=0),
+        functools.partial(bias_kernel, grid),
+        out_shape=pltpu.HBM(bias_shape, f32),
+        in_specs=[HBM],
+        out_specs=HBM,
+        scratch_shapes=[*bias_scratch, pltpu.SemaphoreType.DMA((1,))],
+        compiler_params=pltpu.CompilerParams(vmem_limit_bytes=16 * 2**20),
+        cost_estimate=pl.CostEstimate(
+            flops=4 * 10**6, bytes_accessed=32 * 2**20, transcendentals=0
+        ),
         name="bias",
-    )(jnp.transpose(offset_bias, (0, 2, 1, 3)))
+    )(table)
 
     arrived = {(0, 0): grid_tokens}
     for offset in ORDER:
@@ -279,9 +312,9 @@
     rows, cols = TILES * tile_rows, TILES * tile_cols
     region_rows, region_cols = 2 * tile_rows, 2 * tile_cols
     return pl.pallas_call(
-        layers_kernel,
+        functools.partial(layers_kernel, grid),
         out_shape=jax.ShapeDtypeStruct(grid_tokens.shape, grid_tokens.dtype),
-        in_specs=[VMEM] * (len(tiles) + 1) + [HBM, VMEM, VMEM, HBM, VMEM],
+        in_specs=[VMEM] * (len(tiles) + 1) + [HBM, VMEM, VMEM, HBM, HBM, HBM],
         out_specs=VMEM,
         scratch_shapes=[
             pltpu.VMEM((rows, cols, width), bf16),
@@ -296,9 +329,10 @@
             pltpu.VMEM((SLOTS, QUERIES, SLAB), bf16),
             pltpu.VMEM(w_query.shape, bf16),
             pltpu.VMEM(w_out.shape, bf16),
-            pltpu.SemaphoreType.DMA((2,)),
+            *bias_scratch,
+            pltpu.SemaphoreType.DMA((3,)),
         ],
-        compiler_params=pltpu.CompilerParams(vmem_limit_bytes=24 * 2**20),
+        compiler_params=pltpu.CompilerParams(vmem_limit_bytes=32 * 2**20),
         cost_estimate=pl.CostEstimate(
             flops=6 * 10**9, bytes_accessed=16 * 2**20, transcendentals=10**6
         ),
@@ -310,7 +344,8 @@
         w_key,
         w_value,
         pltpu.with_memory_space_constraint(w_out, pltpu.HBM),
-        bias,
+        table,
+        pltpu.with_memory_space_constraint(bias, pltpu.HBM),
     )
 
 

time: 117 us -> 119 us (1.017)
  Pallas kernels: 9.9 us -> 14.7 us
  waiting for transfers between devices: 7.34 us -> 4.84 us
    pallas_call x2, Pallas kernels: 9.9 us -> 14.7 us  [the longest x1 10.2 us: on_device(): pl.pallas_call(functools.partial(layers_kernel, grid), out_shape=jax.Shap...]
    ppermute x8, waiting for transfers between devices: 7.34 us -> 4.84 us  [from_offset(): return lax.ppermute(cells, ('sp', 'tp'), pairs)]
  transfers between devices with their start and end apart: 8 -> 8, of which waited for: 2 -> 1; matrix products, arithmetic and copies ran while one was open for 0% -> 0% of each run, Pallas kernels for 1% -> 4%
where the time goes in v1:
time: 119 us
  starting transfers between devices  98.9 us (83%)
  Pallas kernels  14.7 us (12%)
  waiting for transfers between devices  4.84 us (4%)
    ppermute x8, starting transfers between devices, from_offset(): return lax.ppermute(cells, ('sp', 'tp'), pairs)  98.9 us
    pallas_call x1, Pallas kernels, on_device(): pl.pallas_call(functools.partial(layers_kernel, grid), out_shape=jax.Shap...  10.2 us
    ppermute x8, waiting for transfers between devices, from_offset(): return lax.ppermute(cells, ('sp', 'tp'), pairs)  4.84 us
    pallas_call x1, Pallas kernels, on_device(): pl.pallas_call(functools.partial(bias_kernel, grid), out_shape=pltpu.HBM(...  4.52 us
  transfers between devices with their start and end apart: 8, of which 1 were waited for; matrix products, arithmetic and copies ran while one was open for 0% of the time, Pallas kernels for 4%

profile of v1, /device:TPU:5, one launch (start us, length us, event | category | flops | bytes accessed | tf_op | source)
XLA Modules:
  0.0 118.6 jit_solution(580121751298260952)
XLA Ops:
  0.0 1.3 %collective-permute-start.6 = (bf16[8,16,1024]{2,1,0:T(8,128)(2,1)}, bf16[8,16,1024]{2,1,0:T(8,128)(2,1)S(1)}, u32[]{:S(2)}, u32[]{:S(2)}) collective-permute-start(bf16[8,16,1024]{2,1,0:T(8,128)(2,1)} %refs_4_.1), channel_id=1, source_target_pairs={{32,0},{33,1},{34,2},{35,3},{36,4},{37,5},{38,6},{39,7},{40,8},{41... | collective-permute-start | bytes 786440 | tf_op jit(solution)/shard_map/ppermute | solution.py:272
  1.3 1.3 %collective-permute-start.5 = (bf16[8,16,1024]{2,1,0:T(8,128)(2,1)}, bf16[8,16,1024]{2,1,0:T(8,128)(2,1)S(1)}, u32[]{:S(2)}, u32[]{:S(2)}) collective-permute-start(bf16[8,16,1024]{2,1,0:T(8,128)(2,1)} %refs_4_.1), channel_id=1, source_target_pairs={{32,1},{33,2},{34,3},{35,4},{36,5},{37,6},{38,7},{39,8},{40,9},{41... | collective-permute-start | bytes 786440 | tf_op jit(solution)/shard_map/ppermute | solution.py:272
  2.6 84.8 %collective-permute-start.4 = (bf16[8,16,1024]{2,1,0:T(8,128)(2,1)}, bf16[8,16,1024]{2,1,0:T(8,128)(2,1)S(1)}, u32[]{:S(2)}, u32[]{:S(2)}) collective-permute-start(bf16[8,16,1024]{2,1,0:T(8,128)(2,1)} %refs_4_.1), channel_id=1, source_target_pairs={{1,0},{2,1},{3,2},{4,3},{5,4},{6,5},{7,6},{8,7},{9,8},{10,9},{11,1... | collective-permute-start | bytes 786440 | tf_op jit(solution)/shard_map/ppermute | solution.py:272
  87.4 2.0 %collective-permute-start.3 = (bf16[8,16,1024]{2,1,0:T(8,128)(2,1)}, bf16[8,16,1024]{2,1,0:T(8,128)(2,1)S(1)}, u32[]{:S(2)}, u32[]{:S(2)}) collective-permute-start(bf16[8,16,1024]{2,1,0:T(8,128)(2,1)} %refs_4_.1), channel_id=1, source_target_pairs={{0,1},{1,2},{2,3},{3,4},{4,5},{5,6},{6,7},{7,8},{8,9},{9,10},{10,1... | collective-permute-start | bytes 786440 | tf_op jit(solution)/shard_map/ppermute | solution.py:272
  89.4 5.4 %collective-permute-start.2 = (bf16[8,16,1024]{2,1,0:T(8,128)(2,1)}, bf16[8,16,1024]{2,1,0:T(8,128)(2,1)S(1)}, u32[]{:S(2)}, u32[]{:S(2)}) collective-permute-start(bf16[8,16,1024]{2,1,0:T(8,128)(2,1)} %refs_4_.1), channel_id=1, source_target_pairs={{1,32},{2,33},{3,34},{4,35},{5,36},{6,37},{7,38},{8,39},{9,40},{10... | collective-permute-start | bytes 786440 | tf_op jit(solution)/shard_map/ppermute | solution.py:272
  94.7 0.0 collective-permute-done.6.refs_7_
  94.7 1.6 %collective-permute-start.1 = (bf16[8,16,1024]{2,1,0:T(8,128)(2,1)}, bf16[8,16,1024]{2,1,0:T(8,128)(2,1)S(1)}, u32[]{:S(2)}, u32[]{:S(2)}) collective-permute-start(bf16[8,16,1024]{2,1,0:T(8,128)(2,1)} %refs_4_.1), channel_id=1, source_target_pairs={{0,32},{1,33},{2,34},{3,35},{4,36},{5,37},{6,38},{7,39},{8,40},{9,... | collective-permute-start | bytes 786440 | tf_op jit(solution)/shard_map/ppermute | solution.py:272
  96.3 0.0 collective-permute-done.5.refs_6_
  96.3 1.3 %collective-permute-start = (bf16[8,16,1024]{2,1,0:T(8,128)(2,1)}, bf16[8,16,1024]{2,1,0:T(8,128)(2,1)S(1)}, u32[]{:S(2)}, u32[]{:S(2)}) collective-permute-start(bf16[8,16,1024]{2,1,0:T(8,128)(2,1)} %refs_4_.1), channel_id=1, source_target_pairs={{0,33},{1,34},{2,35},{3,36},{4,37},{5,38},{6,39},{7,40},{8,41},{9,... | collective-permute-start | bytes 786440 | tf_op jit(solution)/shard_map/ppermute | solution.py:272
  97.6 0.0 collective-permute-done.4.refs_5_
  97.7 1.3 %collective-permute-start.7 = (bf16[8,16,1024]{2,1,0:T(8,128)(2,1)}, bf16[8,16,1024]{2,1,0:T(8,128)(2,1)S(1)}, u32[]{:S(2)}, u32[]{:S(2)}) collective-permute-start(bf16[8,16,1024]{2,1,0:T(8,128)(2,1)} %refs_4_.1), channel_id=1, source_target_pairs={{33,0},{34,1},{35,2},{36,3},{37,4},{38,5},{39,6},{40,7},{41,8},{42... | collective-permute-start | bytes 786440 | tf_op jit(solution)/shard_map/ppermute | solution.py:272
  99.0 0.0 copy-start
  99.0 0.0 copy-start.1
  99.0 0.0 copy-start.2
  99.0 0.0 copy-start.3
  99.0 4.5 %bias.1.refs_15_ = f32[5,4,128,512]{3,2,1,0:T(8,128)} custom-call(f32[2,15,4,31]{3,2,1,0:T(4,128)} %bitcast.1), custom_call_target="tpu_custom_call" | custom-call | flops 4000000 | bytes 33554432 | tf_op jit(solution)/shard_map/bias/pallas_call | solution.py:294
  103.5 0.0 collective-permute-done.3.refs_3_
  103.6 0.0 collective-permute-done.2.refs_2_
  103.6 4.8 %collective-permute-done.1.refs_1_ = bf16[8,16,1024]{2,1,0:T(8,128)(2,1)S(1)} collective-permute-done((bf16[8,16,1024]{2,1,0:T(8,128)(2,1)}, bf16[8,16,1024]{2,1,0:T(8,128)(2,1)S(1)}, u32[]{:S(2)}, u32[]{:S(2)}) %collective-permute-start.1) | collective-permute-done | bytes 262176 | tf_op jit(solution)/shard_map/ppermute | solution.py:272
  108.4 0.0 collective-permute-done.refs_0_
  108.4 0.0 collective-permute-done.7.refs_8_
  108.4 0.0 copy-done
  108.4 0.0 copy-done.1
  108.4 0.0 copy-done.2
  108.4 0.0 copy-done.3
  108.4 10.2 %layers.1 = bf16[8,16,1024]{2,1,0:T(8,128)(2,1)} custom-call(bf16[8,16,1024]{2,1,0:T(8,128)(2,1)S(1)} %collective-permute-done.refs_0_, bf16[8,16,1024]{2,1,0:T(8,128)(2,1)S(1)} %collective-permute-done.1.refs_1_, bf16[8,16,1024]{2,1,0:T(8,128)(2,1)S(1)} %collective-permute-done.2.refs_2_, bf16[8,16,1024]{2,1,0:T(8,128)(2,1)S(1)} %collective-permute-done.3.refs_3_, ...), custom_call_target="tpu_custom_call" | custom-call | flops 6000000000 | bytes 16777216 | tf_op jit(solution)/shard_map/layers/pallas_call | solution.py:314
Async XLA Ops:
  0.0 94.7 %collective-permute-start.6 = (bf16[8,16,1024]{2,1,0:T(8,128)(2,1)}, bf16[8,16,1024]{2,1,0:T(8,128)(2,1)S(1)}, u32[]{:S(2)}, u32[]{:S(2)}) collective-permute-start(bf16[8,16,1024]{2,1,0:T(8,128)(2,1)} %refs_4_.1), channel_id=1, source_target_pairs={{32,0},{33,1},{34,2},{35,3},{36,4},{37,5},{38,6},{39,7},{40,8},{41... | collective-permute-start | bytes 786440 | tf_op jit(solution)/shard_map/ppermute | solution.py:272
  1.3 95.0 %collective-permute-start.5 = (bf16[8,16,1024]{2,1,0:T(8,128)(2,1)}, bf16[8,16,1024]{2,1,0:T(8,128)(2,1)S(1)}, u32[]{:S(2)}, u32[]{:S(2)}) collective-permute-start(bf16[8,16,1024]{2,1,0:T(8,128)(2,1)} %refs_4_.1), channel_id=1, source_target_pairs={{32,1},{33,2},{34,3},{35,4},{36,5},{37,6},{38,7},{39,8},{40,9},{41... | collective-permute-start | bytes 786440 | tf_op jit(solution)/shard_map/ppermute | solution.py:272
  2.6 95.0 %collective-permute-start.4 = (bf16[8,16,1024]{2,1,0:T(8,128)(2,1)}, bf16[8,16,1024]{2,1,0:T(8,128)(2,1)S(1)}, u32[]{:S(2)}, u32[]{:S(2)}) collective-permute-start(bf16[8,16,1024]{2,1,0:T(8,128)(2,1)} %refs_4_.1), channel_id=1, source_target_pairs={{1,0},{2,1},{3,2},{4,3},{5,4},{6,5},{7,6},{8,7},{9,8},{10,9},{11,1... | collective-permute-start | bytes 786440 | tf_op jit(solution)/shard_map/ppermute | solution.py:272
  87.4 16.1 %collective-permute-start.3 = (bf16[8,16,1024]{2,1,0:T(8,128)(2,1)}, bf16[8,16,1024]{2,1,0:T(8,128)(2,1)S(1)}, u32[]{:S(2)}, u32[]{:S(2)}) collective-permute-start(bf16[8,16,1024]{2,1,0:T(8,128)(2,1)} %refs_4_.1), channel_id=1, source_target_pairs={{0,1},{1,2},{2,3},{3,4},{4,5},{5,6},{6,7},{7,8},{8,9},{9,10},{10,1... | collective-permute-start | bytes 786440 | tf_op jit(solution)/shard_map/ppermute | solution.py:272
  89.4 14.2 %collective-permute-start.2 = (bf16[8,16,1024]{2,1,0:T(8,128)(2,1)}, bf16[8,16,1024]{2,1,0:T(8,128)(2,1)S(1)}, u32[]{:S(2)}, u32[]{:S(2)}) collective-permute-start(bf16[8,16,1024]{2,1,0:T(8,128)(2,1)} %refs_4_.1), channel_id=1, source_target_pairs={{1,32},{2,33},{3,34},{4,35},{5,36},{6,37},{7,38},{8,39},{9,40},{10... | collective-permute-start | bytes 786440 | tf_op jit(solution)/shard_map/ppermute | solution.py:272
  94.7 13.6 %collective-permute-start.1 = (bf16[8,16,1024]{2,1,0:T(8,128)(2,1)}, bf16[8,16,1024]{2,1,0:T(8,128)(2,1)S(1)}, u32[]{:S(2)}, u32[]{:S(2)}) collective-permute-start(bf16[8,16,1024]{2,1,0:T(8,128)(2,1)} %refs_4_.1), channel_id=1, source_target_pairs={{0,32},{1,33},{2,34},{3,35},{4,36},{5,37},{6,38},{7,39},{8,40},{9,... | collective-permute-start | bytes 786440 | tf_op jit(solution)/shard_map/ppermute | solution.py:272
  96.3 12.1 %collective-permute-start = (bf16[8,16,1024]{2,1,0:T(8,128)(2,1)}, bf16[8,16,1024]{2,1,0:T(8,128)(2,1)S(1)}, u32[]{:S(2)}, u32[]{:S(2)}) collective-permute-start(bf16[8,16,1024]{2,1,0:T(8,128)(2,1)} %refs_4_.1), channel_id=1, source_target_pairs={{0,33},{1,34},{2,35},{3,36},{4,37},{5,38},{6,39},{7,40},{8,41},{9,... | collective-permute-start | bytes 786440 | tf_op jit(solution)/shard_map/ppermute | solution.py:272
  97.7 10.7 %collective-permute-start.7 = (bf16[8,16,1024]{2,1,0:T(8,128)(2,1)}, bf16[8,16,1024]{2,1,0:T(8,128)(2,1)S(1)}, u32[]{:S(2)}, u32[]{:S(2)}) collective-permute-start(bf16[8,16,1024]{2,1,0:T(8,128)(2,1)} %refs_4_.1), channel_id=1, source_target_pairs={{33,0},{34,1},{35,2},{36,3},{37,4},{38,5},{39,6},{40,7},{41,8},{42... | collective-permute-start | bytes 786440 | tf_op jit(solution)/shard_map/ppermute | solution.py:272
  99.0 9.4 %copy-start = (bf16[2,1024,512]{2,1,0:T(8,128)(2,1)S(1)}, bf16[2,1024,512]{2,1,0:T(8,128)(2,1)}, u32[]{:S(2)}) copy-start(bf16[2,1024,512]{2,1,0:T(8,128)(2,1)} %refs_11_.1) | copy-start | bytes 6291460
  99.0 9.4 %copy-start.1 = (bf16[2,1024,512]{2,1,0:T(8,128)(2,1)S(1)}, bf16[2,1024,512]{2,1,0:T(8,128)(2,1)}, u32[]{:S(2)}) copy-start(bf16[2,1024,512]{2,1,0:T(8,128)(2,1)} %refs_12_.1) | copy-start | bytes 6291460
  99.0 9.4 %copy-start.2 = (bf16[8,16,1024]{2,1,0:T(8,128)(2,1)S(1)}, bf16[8,16,1024]{2,1,0:T(8,128)(2,1)}, u32[]{:S(2)}) copy-start(bf16[8,16,1024]{2,1,0:T(8,128)(2,1)} %refs_4_.1) | copy-start | bytes 786436
  99.0 9.4 %copy-start.3 = (f32[2,1024]{1,0:T(2,128)S(1)}, f32[2,1024]{1,0:T(2,128)}, u32[]{:S(2)}) copy-start(f32[2,1024]{1,0:T(2,128)} %refs_9_.1) | copy-start | bytes 24580
